TPU v7x, 32 devices: a whole 2x2x4 slice. The times are simulated.
32 devices in a mesh: sp: 8 (over z, y), tp: 4 (over x, core).
Axes of the slice: x: 2, y: 2, z: 4, core: 2. Of those that a mesh axis runs over, the one named last changes fastest.
Arguments:
- queries: bfloat16 [4096, 1024], P('sp', 'tp'), may hold values from -200 to 200
- keys: bfloat16 [4096, 1024], P('sp', 'tp'), may hold values from -6 to 6
- values: bfloat16 [4096, 1024], P('sp', 'tp'), may hold values from -24 to 24
- cum_gate: float32 [4096, 8], P('sp', 'tp'), may hold values from -414 to 0, as said below
- residual: bfloat16 [4096, 2048], P(('sp', 'tp')), may hold values from -1.5 to 1.5
- w_out: bfloat16 [1024, 2048], replicated, may hold values from -0.1875 to 0.1875
- gain: float32 [2048], replicated, may hold values from 0.1 to 1.9
- w_up: bfloat16 [2048, 8192], P('sp', 'tp'), may hold values from -0.125 to 0.125
- w_down: bfloat16 [8192, 2048], P('tp', 'sp'), may hold values from -0.0625 to 0.0625
Outputs:
- output: bfloat16 [4096, 2048], P(('sp', 'tp'))
Inputs may be any that keep to these rules, and one draw needn't show every extreme that they name: Within each head, cum_gate never rises from one position to the next.
All inputs are finite; a program needn't handle non-finite values.
Results may differ from a plain program's by a relative error of at most 0.022.
Values may be sent and summed in bfloat16 or wider, within the bound.
A program may use at most 128 MiB of HBM per device.

v0:
```python
import math
import jax
import jax.numpy as jnp
from jax import lax
from jax.sharding import PartitionSpec as P


def per_device(queries, keys, values, cum_gate, residual, w_out, gain, w_up, w_down):
    tok_rows, width = queries.shape
    heads_here = cum_gate.shape[1]
    head_size = width // heads_here
    score_scale = head_size ** (-0.5)
    row_offset = lax.axis_index("sp") * tok_rows
    query_heads = queries.reshape(tok_rows, heads_here, head_size)
    query_pos = row_offset + jnp.arange(tok_rows, dtype=jnp.int32)
    all_gates = lax.all_gather(cum_gate, "sp", axis=0, tiled=True)
    initial = (
        jnp.full((tok_rows, heads_here), -1e30, jnp.float32),
        jnp.zeros((tok_rows, heads_here), jnp.float32),
        jnp.zeros((tok_rows, heads_here, head_size), jnp.float32),
    )
    carried = initial
    key_rows = lax.all_gather(keys, "sp", axis=0, tiled=True)
    value_rows = lax.all_gather(values, "sp", axis=0, tiled=True)
    row_count = key_rows.shape[0]
    span_rows = math.gcd(row_count, 2048)
    block_count = row_count // span_rows
    key_blocks = key_rows.reshape(block_count, span_rows, heads_here, head_size)
    value_blocks = value_rows.reshape(block_count, span_rows, heads_here, head_size)
    first_pos = jnp.arange(block_count, dtype=jnp.int32) * span_rows

    def absorb_block(running, packed):
        running_max, running_sum, accumulated = running
        key_blk, value_blk, block_start = packed
        gate_blk = lax.dynamic_slice_in_dim(all_gates, block_start, span_rows, 0)
        scores = jnp.einsum(
            "qhd,khd->qhk", query_heads, key_blk, preferred_element_type=jnp.float32
        )
        scores = scores * score_scale + cum_gate[:, :, None] - gate_blk.T[None, :, :]
        key_pos = block_start + jnp.arange(span_rows, dtype=jnp.int32)
        scores = jnp.where(key_pos[None, None, :] <= query_pos[:, None, None], scores, -1e30)
        new_max = jnp.maximum(running_max, jnp.max(scores, axis=-1))
        rescale = jnp.exp(running_max - new_max)
        weights = jnp.exp(scores - new_max[:, :, None])
        running_sum = running_sum * rescale + jnp.sum(weights, axis=-1)
        product = jnp.einsum(
            "qhk,khd->qhd",
            weights.astype(jnp.bfloat16),
            value_blk,
            preferred_element_type=jnp.float32,
        )
        accumulated = accumulated * rescale[:, :, None] + product
        return ((new_max, running_sum, accumulated), None)

    carried, _ = lax.scan(absorb_block, carried, (key_blocks, value_blocks, first_pos))
    running_max, running_sum, accumulated = carried
    attended = (accumulated / running_sum[:, :, None]).reshape(tok_rows, width).astype(jnp.bfloat16)
    mine = lax.all_to_all(attended, "tp", split_axis=0, concat_axis=1, tiled=True)
    projected = jnp.dot(mine, w_out, preferred_element_type=jnp.float32)
    residual_sum = residual.astype(jnp.float32) + projected
    mean_square = jnp.mean(residual_sum * residual_sum, axis=-1, keepdims=True)
    normed = (residual_sum * lax.rsqrt(mean_square + 1e-06) * gain).astype(jnp.bfloat16)
    normed_all = lax.all_gather(normed, "tp", axis=0, tiled=True)
    up_proj = jnp.dot(
        normed_all,
        lax.all_gather(w_up, "sp", axis=0, tiled=True),
        preferred_element_type=jnp.float32,
    )
    hidden = jnp.square(jax.nn.relu(up_proj)).astype(jnp.bfloat16)
    down_whole = lax.all_gather(w_down, "sp", axis=1, tiled=True)
    rounded = jnp.dot(hidden, down_whole, preferred_element_type=jnp.float32).astype(jnp.bfloat16)
    branch_out = lax.psum_scatter(
        lax.optimization_barrier(rounded).astype(jnp.float32).astype(jnp.bfloat16),
        "tp",
        scatter_dimension=0,
        tiled=True,
    ).astype(jnp.float32)
    return (residual_sum + branch_out).astype(jnp.bfloat16)


def solution(mesh):
    return jax.shard_map(
        per_device,
        mesh=mesh,
        in_specs=(
            P("sp", "tp"),
            P("sp", "tp"),
            P("sp", "tp"),
            P("sp", "tp"),
            P(("sp", "tp"), None),
            P(),
            P(),
            P("sp", "tp"),
            P("tp", "sp"),
        ),
        out_specs=P(("sp", "tp"), None),
        check_vma=False,
    )
```

profile of v0, /device:TPU:0, one launch (start us, length us, event | category | flops | bytes accessed | tf_op | source)
XLA Modules:
  0.0 501.9 jit_solution(15590965651173478988)
XLA Ops:
  6.5 0.0 copy-start
  6.5 0.0 all-gather.6.cloned.1.call-start
  6.5 0.7 all-gather.6.cloned.1.call-update
  7.3 0.0 all-gather.8.cloned.1.call-start
  7.3 0.7 all-gather.8.cloned.1.call-update
  8.0 0.0 all-gather.10.cloned.1.call-start
  8.1 1.1 copy.17
  9.2 0.2 copy.19
  9.4 32.7 %all_gather.19 = f32[4096,2]{0,1:T(2,128)S(1)} all-gather(f32[512,2]{0,1:T(2,128)} %param.14), channel_id=1, replica_groups=mesh['sp'=8,'tp'=4] {'sp'}, dimensions={0}, use_global_device_ids=true | all-gather | bytes 36864 | tf_op jit(solution)/shard_map/all_gather | solution.py:16
  42.0 19.4 %all-gather.6.cloned.1.call-done = bf16[4096,256]{1,0:T(8,128)(2,1)} async-done(((bf16[512,256]{1,0:T(8,128)(2,1)}), bf16[4096,256]{1,0:T(8,128)(2,1)}) %all-gather.6.cloned.1.call-update) | async-done | bytes 2097168 | tf_op jit(solution)/shard_map/all_gather | solution.py:23
  61.4 4.0 reshape.62
  65.4 45.8 %all-gather.8.cloned.1.call-done = bf16[4096,256]{1,0:T(8,128)(2,1)} async-done(((bf16[512,256]{1,0:T(8,128)(2,1)}), bf16[4096,256]{1,0:T(8,128)(2,1)}) %all-gather.8.cloned.1.call-update) | async-done | bytes 2097168 | tf_op jit(solution)/shard_map/all_gather | solution.py:24
  111.2 4.0 reshape.64
  115.2 0.0 copy-done
  115.2 45.9 %while.15 = (s32[]{:T(128)}, f32[512,2]{0,1:T(2,128)S(1)}, f32[512,2]{0,1:T(2,128)S(1)}, f32[512,2,128]{0,2,1:T(8,128)}, s32[2]{0:T(128)S(1)}, /*index=5*/bf16[2...) while((s32[]{:T(128)}, f32[512,2]{0,1:T(2,128)S(1)}, ...), condition=%wide.region_3.4_spmd.clone, body=%wide.region_0.3_spmd.clone.sunk | while | flops 1110842880 | bytes 39239884 | solution.py:55
  115.2 0.6 dynamic_slice.26
  117.4 0.1 dynamic-slice_bitcast_fusion.2
  117.5 0.6 iota_add_fusion.5
  118.1 0.8 broadcast_compare_fusion.2
  118.9 2.7 constant_dynamic-slice_fusion.3
  121.6 4.6 fusion.40
  126.2 4.8 fusion.42
  131.0 0.8 copy.34
  131.8 6.2 %fusion.44 = f32[512,2,128]{0,2,1:T(8,128)} fusion(f32[2,2048,512]{2,1,0:T(8,128)} %get-tuple-element.231, f32[512,2]{0,1:T(2,128)S(1)} %fusion.41, f32[2,2048]{1,0:T(2,128)S(1)} %dynamic-slice_bitcast_fusion.2, f32[512,2]{0,1:T(2,128)S(1)} %get-tuple-element.270, pred[512,2048]{0,1:T(8,128)(4,1)S(1)} %broadcast_compare_fusion.2, ...), kind=kOutput, calls=%fused_computation.12.clone.1 | convolution fusion | flops 549847040 | bytes 11563009 | tf_op jit(solution)/shard_map/while/body/eval_jaxpr/qhk,khd->qhd/dot_general | solution.py:46
  138.1 0.6 dynamic_slice.26
  140.3 0.1 dynamic-slice_bitcast_fusion.2
  140.4 0.6 iota_add_fusion.5
  141.0 0.8 broadcast_compare_fusion.2
  141.8 2.7 constant_dynamic-slice_fusion.3
  144.5 4.6 fusion.40
  149.1 4.8 fusion.42
  153.9 0.8 copy.34
  154.7 6.4 %fusion.44 = f32[512,2,128]{0,2,1:T(8,128)} fusion(f32[2,2048,512]{2,1,0:T(8,128)} %get-tuple-element.231, f32[512,2]{0,1:T(2,128)S(1)} %fusion.41, f32[2,2048]{1,0:T(2,128)S(1)} %dynamic-slice_bitcast_fusion.2, f32[512,2]{0,1:T(2,128)S(1)} %get-tuple-element.270, pred[512,2048]{0,1:T(8,128)(4,1)S(1)} %broadcast_compare_fusion.2, ...), kind=kOutput, calls=%fused_computation.12.clone.1 | convolution fusion | flops 549847040 | bytes 11563009 | tf_op jit(solution)/shard_map/while/body/eval_jaxpr/qhk,khd->qhd/dot_general | solution.py:46
  161.1 0.0 copy-start.1
  161.1 1.1 divide_convert_fusion
  162.2 0.1 reshape.65
  162.2 0.2 copy.24
  162.4 8.5 %all_to_all.16 = bf16[4,128,256]{2,1,0:T(8,128)(2,1)S(1)} all-to-all(bf16[4,128,256]{2,1,0:T(8,128)(2,1)S(1)} %copy.24), channel_id=1, replica_groups=mesh['sp'=8,'tp'=4] {'tp'}, dimensions={0} | all-to-all | bytes 524288 | tf_op jit(solution)/shard_map/all_to_all | solution.py:58
  171.0 0.2 copy.22
  171.1 3.1 multiply_reduce_fusion
  174.3 0.0 copy-done.1
  174.3 0.9 multiply_convert_fusion.1
  175.2 0.0 all-gather.10.cloned.1.call-update
  175.3 0.0 all-gather.12.cloned.1.call-start
  175.3 0.5 all-gather.12.cloned.1.call-update
  175.8 0.0 all-gather.14.cloned.1.call-start
  175.9 0.5 all-gather.14.cloned.1.call-update
  176.4 0.2 reduce-scatter.2.cloned.1.call-start
  176.7 19.0 %all-gather.10.cloned.1.call-done = bf16[512,2048]{1,0:T(8,128)(2,1)} async-done(((bf16[128,2048]{1,0:T(8,128)(2,1)}), bf16[512,2048]{1,0:T(8,128)(2,1)}) %all-gather.10.cloned.1.call-update) | async-done | bytes 2097168 | tf_op jit(solution)/shard_map/all_gather | solution.py:63
  195.6 126.5 %all-gather.12.cloned.1.call-done = bf16[2048,2048]{1,0:T(8,128)(2,1)} async-done(((bf16[256,2048]{1,0:T(8,128)(2,1)}), bf16[2048,2048]{1,0:T(8,128)(2,1)}) %all-gather.12.cloned.1.call-update) | async-done | bytes 8388624 | tf_op jit(solution)/shard_map/all_gather | solution.py:66
  322.1 125.0 %all-gather.14.cloned.1.call-done = bf16[2048,2048]{1,0:T(8,128)(2,1)} async-done(((bf16[2048,256]{1,0:T(8,128)(2,1)}), bf16[2048,2048]{1,0:T(8,128)(2,1)}) %all-gather.14.cloned.1.call-update) | async-done | bytes 8388624 | tf_op jit(solution)/shard_map/all_gather | solution.py:70
  447.1 16.5 %convolution_convert_fusion = bf16[512,2048]{1,0:T(8,128)(2,1)} fusion(bf16[2048,2048]{1,0:T(8,128)(2,1)} %all-gather.14.cloned.1.call-done, bf16[512,2048]{1,0:T(8,128)(2,1)} %all-gather.10.cloned.1.call-done, bf16[2048,2048]{1,0:T(8,128)(2,1)} %all-gather.12.cloned.1.call-done), kind=kOutput, calls=%fused_computation.30 | convolution fusion | flops 8594128896 | bytes 20971520 | tf_op jit(solution)/shard_map/dot_general | solution.py:71
  463.7 0.0 reduce-scatter.2.cloned.1.call-update
  463.7 29.5 %reduce-scatter.2.cloned.1.call-done = bf16[128,2048]{1,0:T(8,128)(2,1)} async-done(((bf16[512,2048]{1,0:T(8,128)(2,1)}), bf16[128,2048]{1,0:T(8,128)(2,1)}) %reduce-scatter.2.cloned.1.call-update) | async-done | bytes 524304 | tf_op jit(solution)/shard_map/reduce_scatter | solution.py:72
  493.2 1.9 add_convert_fusion
  (13 shorter events, 0.1 us)
Async XLA Ops:
  6.5 108.6 %copy-start = (f32[512,2]{0,1:T(2,128)S(1)}, f32[512,2]{0,1:T(2,128)}, u32[]{:S(2)}) copy-start(f32[512,2]{0,1:T(2,128)} %param.14) | copy-start | bytes 12292
  6.5 54.9 %all-gather.6.cloned.1.call-start = ((), (), s32[]{:S(2)}) async-start(), calls=%async_computation.2 | async-start | bytes 2359296 | tf_op jit(solution)/shard_map/all_gather | solution.py:23
  7.3 103.9 %all-gather.8.cloned.1.call-start = ((), (), s32[]{:S(2)}) async-start(), calls=%async_computation.3 | async-start | bytes 2359296 | tf_op jit(solution)/shard_map/all_gather | solution.py:24
  8.0 187.6 %all-gather.10.cloned.1.call-start = ((), (), s32[]{:S(2)}) async-start(), calls=%async_computation.4 | async-start | bytes 2621440 | tf_op jit(solution)/shard_map/all_gather | solution.py:63
  161.1 13.2 %copy-start.1 = (f32[2048]{0:T(1024)S(1)}, f32[2048]{0:T(1024)}, u32[]{:S(2)}) copy-start(f32[2048]{0:T(1024)} %param.17) | copy-start | bytes 24580
  175.3 146.8 %all-gather.12.cloned.1.call-start = ((), (), s32[]{:S(2)}) async-start(), calls=%async_computation.5 | async-start | bytes 9437184 | tf_op jit(solution)/shard_map/all_gather | solution.py:66
  175.8 271.3 %all-gather.14.cloned.1.call-start = ((), (), s32[]{:S(2)}) async-start(), calls=%async_computation.6 | async-start | bytes 9437184 | tf_op jit(solution)/shard_map/all_gather | solution.py:70
  176.4 316.7 %reduce-scatter.2.cloned.1.call-start = ((), (), s32[]{:S(2)}) async-start(), calls=%async_computation.7 | async-start | bytes 2621440 | tf_op jit(solution)/shard_map/reduce_scatter | solution.py:72
Sparse Core Ops, SparseCore 0:
  9.5 51.9 all-gather.5
  63.5 47.6 all-gather.7
  175.4 20.1 all-gather.9
  197.6 124.4 all-gather.11
  324.0 123.1 all-gather.13
  463.8 29.3 reduce-scatter.1
where the time goes:
time: 502 us
  waiting for transfers between devices  368 us (73%)
  matrix products  41.4 us (8%)
  blocking collectives  41.2 us (8%)
  local copies, waits for them, and re-layouts  18 us (4%)
  other arithmetic  16.3 us (3%)
  between operations  13.6 us (3%)
    all_gather x1, waiting for transfers between devices, per_device(): lax.all_gather(w_up, 'sp', axis=0, tiled=True)  126 us
    all_gather x1, waiting for transfers between devices, per_device(): down_whole = lax.all_gather(w_down, 'sp', axis=1, tiled=True)  125 us
    all_gather x1, waiting for transfers between devices, per_device(): value_rows = lax.all_gather(values, 'sp', axis=0, tiled=True)  45.8 us
    all_gather x1, blocking collectives, per_device(): all_gates = lax.all_gather(cum_gate, 'sp', axis=0, tiled=True)  32.7 us
    reduce_scatter x1, waiting for transfers between devices, per_device(): lax.psum_scatter(lax.optimization_barrier(rounded).astype(jnp.float32).as...  29.5 us
    all_gather x1, waiting for transfers between devices, per_device(): key_rows = lax.all_gather(keys, 'sp', axis=0, tiled=True)  19.4 us
    all_gather x1, waiting for transfers between devices, per_device(): normed_all = lax.all_gather(normed, 'tp', axis=0, tiled=True)  19 us
    dot_general x1, matrix products, per_device(): jnp.dot(hidden, down_whole, preferred_element_type=jnp.float32)  16.5 us
  transfers between devices with their start and end apart: 6, of which 6 were waited for; matrix products, arithmetic and copies ran while one was open for 1% of the time, Pallas kernels for 0%

commit v1 on v0

--- a/solution.py
+++ b/solution.py
@@ -3,6 +3,16 @@
 import jax.numpy as jnp
 from jax import lax
 from jax.sharding import PartitionSpec as P
+
+
+def fix_keys(matrix, panel, lane_axis):
+    return jnp.split(
+        jax.lax.all_gather(
+            jnp.concatenate([matrix, panel], 1), axis=0, axis_name=lane_axis, tiled=True
+        ),
+        [matrix.shape[1]],
+        axis=1,
+    )
 
 
 def per_device(queries, keys, values, cum_gate, residual, w_out, gain, w_up, w_down):
@@ -13,14 +23,13 @@
     row_offset = lax.axis_index("sp") * tok_rows
     query_heads = queries.reshape(tok_rows, heads_here, head_size)
     query_pos = row_offset + jnp.arange(tok_rows, dtype=jnp.int32)
-    all_gates = lax.all_gather(cum_gate, "sp", axis=0, tiled=True)
     initial = (
         jnp.full((tok_rows, heads_here), -1e30, jnp.float32),
         jnp.zeros((tok_rows, heads_here), jnp.float32),
         jnp.zeros((tok_rows, heads_here, head_size), jnp.float32),
     )
     carried = initial
-    key_rows = lax.all_gather(keys, "sp", axis=0, tiled=True)
+    all_gates, key_rows = fix_keys(cum_gate, keys, "sp")
     value_rows = lax.all_gather(values, "sp", axis=0, tiled=True)
     row_count = key_rows.shape[0]
     span_rows = math.gcd(row_count, 2048)

time: 502 us -> 547 us (1.090)
  waiting for transfers between devices: 368 us -> 423 us
  blocking collectives: 41.2 us -> 8.55 us
  local copies, waits for them, and re-layouts: 18 us -> 33.6 us
    all_gather x1, waiting for transfers between devices: 19.4 us -> 71.2 us  [fix_keys(): jax.lax.all_gather(jnp.concatenate([matrix, panel], 1), axis=0, axis_name...]
    all_gather x1 -> x0, blocking collectives: 32.7 us -> none  [per_device(): all_gates = lax.all_gather(cum_gate, 'sp', axis=0, tiled=True)]
    dynamic_slice x6 -> x10, local copies, waits for them, and re-layouts: 8.16 us -> 21.1 us  [per_device(): lax.scan(absorb_block, carried, (key_blocks, value_blocks, first_pos))]
where the time goes in v1:
time: 547 us; the launch traced here: 546 us
  waiting for transfers between devices  423 us (77%)
  matrix products  45.5 us (8%)
  local copies, waits for them, and re-layouts  33.6 us (6%)
  other arithmetic  18 us (3%)
  between operations  13.6 us (2%)
  blocking collectives  8.55 us (2%)
    all_gather x1, waiting for transfers between devices, per_device(): lax.all_gather(w_up, 'sp', axis=0, tiled=True)  126 us
    all_gather x1, waiting for transfers between devices, per_device(): down_whole = lax.all_gather(w_down, 'sp', axis=1, tiled=True)  125 us
    all_gather x1, waiting for transfers between devices, fix_keys(): jax.lax.all_gather(jnp.concatenate([matrix, panel], 1), axis=0, axis_name...  71.2 us
    all_gather x1, waiting for transfers between devices, per_device(): value_rows = lax.all_gather(values, 'sp', axis=0, tiled=True)  49.9 us
    reduce_scatter x1, waiting for transfers between devices, per_device(): lax.psum_scatter(lax.optimization_barrier(rounded).astype(jnp.float32).as...  29.5 us
    dynamic_slice x10, local copies, waits for them, and re-layouts, per_device(): lax.scan(absorb_block, carried, (key_blocks, value_blocks, first_pos))  21.1 us
    all_gather x1, waiting for transfers between devices, per_device(): normed_all = lax.all_gather(normed, 'tp', axis=0, tiled=True)  19.1 us
    dot_general x1, matrix products, per_device(): jnp.dot(hidden, down_whole, preferred_element_type=jnp.float32)  16.5 us
  transfers between devices with their start and end apart: 6, of which 6 were waited for; matrix products, arithmetic and copies ran while one was open for 1% of the time, Pallas kernels for 0%

profile of v1, /device:TPU:0, one launch (start us, length us, event | category | flops | bytes accessed | tf_op | source)
XLA Modules:
  0.0 546.1 jit_solution(1133121253935521033)
XLA Ops:
  6.5 0.0 all-gather.8.cloned.1.call-start
  6.5 0.0 copy-start
  6.5 0.7 all-gather.8.cloned.1.call-update
  7.3 0.0 all-gather.6.cloned.1.call-start
  7.3 1.1 copy.20
  8.4 0.1 convert_element_type.34
  8.5 1.5 pad_maximum_fusion
  10.0 0.0 all-gather.6.cloned.1.call-update
  10.0 0.0 all-gather.10.cloned.1.call-start
  10.1 1.1 copy.22
  11.2 0.2 copy.24
  11.4 49.9 %all-gather.8.cloned.1.call-done = bf16[4096,256]{1,0:T(8,128)(2,1)} async-done(((bf16[512,256]{1,0:T(8,128)(2,1)}), bf16[4096,256]{1,0:T(8,128)(2,1)}) %all-gather.8.cloned.1.call-update) | async-done | bytes 2097168 | tf_op jit(solution)/shard_map/all_gather | solution.py:33
  61.3 4.0 reshape.64
  65.3 71.2 %all-gather.6.cloned.1.call-done = f32[4096,258]{0,1:T(8,128)} async-done(((f32[512,258]{0,1:T(8,128)}), f32[4096,258]{0,1:T(8,128)}) %all-gather.6.cloned.1.call-update) | async-done | bytes 4227088 | tf_op jit(solution)/shard_map/all_gather | solution.py:10
  136.5 0.0 slice-start
  136.5 2.7 split.8
  139.2 2.8 reshape.65
  142.0 0.0 copy-done
  142.0 0.0 slice-done
  142.0 63.3 %while.15 = (s32[]{:T(128)}, f32[512,2]{0,1:T(2,128)S(1)}, f32[512,2]{0,1:T(2,128)S(1)}, f32[512,2,128]{0,2,1:T(8,128)}, s32[2]{0:T(128)S(1)}, /*index=5*/bf16[2...) while((s32[]{:T(128)}, f32[512,2]{0,1:T(2,128)S(1)}, ...), condition=%wide.region_3.4_spmd.clone, body=%wide.region_0.3_spmd.clone.sunk | while | flops 1110842880 | bytes 41337040 | solution.py:64
  142.0 0.6 dynamic_slice.29
  144.4 0.1 dynamic-slice_bitcast_fusion.2
  144.5 0.6 iota_add_fusion.5
  145.1 0.8 broadcast_compare_fusion.2
  145.9 3.8 constant_dynamic-slice_fusion.4
  149.7 3.6 copy.36
  153.2 6.6 %fusion.41 = (f32[512,2]{0,1:T(2,128)S(1)}, f32[2,2048,512]{2,1,0:T(8,128)}) fusion(f32[2,2048]{1,0:T(2,128)S(1)} %dynamic-slice_bitcast_fusion.2, f32[512,2]{0,1:T(2,128)S(1)} %get-tuple-element.264, pred[512,2048]{0,1:T(8,128)(4,1)S(1)} %broadcast_compare_fusion.2, bf16[512,2,128]{2,0,1:T(8,128)(2,1)S(1)} %get-tuple-element.263, ...), kind=kOutput, calls=%fused_computation.7.clone.1 | convolution fusion | flops 547355648 | bytes 10772480 | tf_op jit(solution)/shard_map/while/body/eval_jaxpr/qhd,khd->qhk/dot_general | solution.py:45
  159.9 4.8 fusion.43
  164.7 1.8 constant_dynamic-slice_fusion.5
  166.5 0.8 copy.37
  167.3 6.2 %fusion.45 = f32[512,2,128]{0,2,1:T(8,128)} fusion(f32[2,2048,512]{2,1,0:T(8,128)} %get-tuple-element.226, f32[512,2]{0,1:T(2,128)S(1)} %fusion.42, f32[2,2048]{1,0:T(2,128)S(1)} %dynamic-slice_bitcast_fusion.2, f32[512,2]{0,1:T(2,128)S(1)} %get-tuple-element.264, pred[512,2048]{0,1:T(8,128)(4,1)S(1)} %broadcast_compare_fusion.2, ...), kind=kOutput, calls=%fused_computation.14.clone.1 | convolution fusion | flops 549847040 | bytes 11563009 | tf_op jit(solution)/shard_map/while/body/eval_jaxpr/qhk,khd->qhd/dot_general | solution.py:55
  173.6 0.6 dynamic_slice.29
  176.0 0.1 dynamic-slice_bitcast_fusion.2
  176.1 0.6 iota_add_fusion.5
  176.7 0.8 broadcast_compare_fusion.2
  177.5 3.8 constant_dynamic-slice_fusion.4
  181.2 3.6 copy.36
  184.8 6.6 %fusion.41 = (f32[512,2]{0,1:T(2,128)S(1)}, f32[2,2048,512]{2,1,0:T(8,128)}) fusion(f32[2,2048]{1,0:T(2,128)S(1)} %dynamic-slice_bitcast_fusion.2, f32[512,2]{0,1:T(2,128)S(1)} %get-tuple-element.264, pred[512,2048]{0,1:T(8,128)(4,1)S(1)} %broadcast_compare_fusion.2, bf16[512,2,128]{2,0,1:T(8,128)(2,1)S(1)} %get-tuple-element.263, ...), kind=kOutput, calls=%fused_computation.7.clone.1 | convolution fusion | flops 547355648 | bytes 10772480 | tf_op jit(solution)/shard_map/while/body/eval_jaxpr/qhd,khd->qhk/dot_general | solution.py:45
  191.5 4.8 fusion.43
  196.3 1.8 constant_dynamic-slice_fusion.5
  198.1 0.8 copy.37
  198.9 6.4 %fusion.45 = f32[512,2,128]{0,2,1:T(8,128)} fusion(f32[2,2048,512]{2,1,0:T(8,128)} %get-tuple-element.226, f32[512,2]{0,1:T(2,128)S(1)} %fusion.42, f32[2,2048]{1,0:T(2,128)S(1)} %dynamic-slice_bitcast_fusion.2, f32[512,2]{0,1:T(2,128)S(1)} %get-tuple-element.264, pred[512,2048]{0,1:T(8,128)(4,1)S(1)} %broadcast_compare_fusion.2, ...), kind=kOutput, calls=%fused_computation.14.clone.1 | convolution fusion | flops 549847040 | bytes 11563009 | tf_op jit(solution)/shard_map/while/body/eval_jaxpr/qhk,khd->qhd/dot_general | solution.py:55
  205.3 0.0 copy-start.1
  205.3 1.1 divide_convert_fusion
  206.4 0.1 reshape.66
  206.4 0.2 copy.31
  206.6 8.5 %all_to_all.16 = bf16[4,128,256]{2,1,0:T(8,128)(2,1)S(1)} all-to-all(bf16[4,128,256]{2,1,0:T(8,128)(2,1)S(1)} %copy.31), channel_id=1, replica_groups=mesh['sp'=8,'tp'=4] {'tp'}, dimensions={0} | all-to-all | bytes 524288 | tf_op jit(solution)/shard_map/all_to_all | solution.py:67
  215.2 0.2 copy.27
  215.3 3.1 multiply_reduce_fusion
  218.5 0.0 copy-done.1
  218.5 0.9 multiply_convert_fusion.1
  219.4 0.0 all-gather.10.cloned.1.call-update
  219.5 0.0 all-gather.12.cloned.1.call-start
  219.5 0.5 all-gather.12.cloned.1.call-update
  220.0 0.0 all-gather.14.cloned.1.call-start
  220.1 0.5 all-gather.14.cloned.1.call-update
  220.6 0.0 reduce-scatter.2.cloned.1.call-start
  220.7 19.1 %all-gather.10.cloned.1.call-done = bf16[512,2048]{1,0:T(8,128)(2,1)} async-done(((bf16[128,2048]{1,0:T(8,128)(2,1)}), bf16[512,2048]{1,0:T(8,128)(2,1)}) %all-gather.10.cloned.1.call-update) | async-done | bytes 2097168 | tf_op jit(solution)/shard_map/all_gather | solution.py:72
  239.8 126.5 %all-gather.12.cloned.1.call-done = bf16[2048,2048]{1,0:T(8,128)(2,1)} async-done(((bf16[256,2048]{1,0:T(8,128)(2,1)}), bf16[2048,2048]{1,0:T(8,128)(2,1)}) %all-gather.12.cloned.1.call-update) | async-done | bytes 8388624 | tf_op jit(solution)/shard_map/all_gather | solution.py:75
  366.3 125.0 %all-gather.14.cloned.1.call-done = bf16[2048,2048]{1,0:T(8,128)(2,1)} async-done(((bf16[2048,256]{1,0:T(8,128)(2,1)}), bf16[2048,2048]{1,0:T(8,128)(2,1)}) %all-gather.14.cloned.1.call-update) | async-done | bytes 8388624 | tf_op jit(solution)/shard_map/all_gather | solution.py:79
  491.3 16.5 %convolution_convert_fusion = bf16[512,2048]{1,0:T(8,128)(2,1)} fusion(bf16[2048,2048]{1,0:T(8,128)(2,1)} %all-gather.14.cloned.1.call-done, bf16[512,2048]{1,0:T(8,128)(2,1)} %all-gather.10.cloned.1.call-done, bf16[2048,2048]{1,0:T(8,128)(2,1)} %all-gather.12.cloned.1.call-done), kind=kOutput, calls=%fused_computation.30 | convolution fusion | flops 8594128896 | bytes 20971520 | tf_op jit(solution)/shard_map/dot_general | solution.py:80
  507.8 0.0 reduce-scatter.2.cloned.1.call-update
  507.9 29.5 %reduce-scatter.2.cloned.1.call-done = bf16[128,2048]{1,0:T(8,128)(2,1)} async-done(((bf16[512,2048]{1,0:T(8,128)(2,1)}), bf16[128,2048]{1,0:T(8,128)(2,1)}) %reduce-scatter.2.cloned.1.call-update) | async-done | bytes 524304 | tf_op jit(solution)/shard_map/reduce_scatter | solution.py:81
  537.3 1.9 add_convert_fusion
  (13 shorter events, 0.1 us)
Async XLA Ops:
  6.5 54.8 %all-gather.8.cloned.1.call-start = ((), (), s32[]{:S(2)}) async-start(), calls=%async_computation.3 | async-start | bytes 2359296 | tf_op jit(solution)/shard_map/all_gather | solution.py:33
  6.5 135.4 %copy-start = (f32[512,2]{0,1:T(2,128)S(1)}, f32[512,2]{0,1:T(2,128)}, u32[]{:S(2)}) copy-start(f32[512,2]{0,1:T(2,128)} %param.14) | copy-start | bytes 12292
  7.3 129.2 %all-gather.6.cloned.1.call-start = ((), (), s32[]{:S(2)}) async-start(), calls=%async_computation.2 | async-start | bytes 4866048 | tf_op jit(solution)/shard_map/all_gather | solution.py:10
  10.0 229.7 %all-gather.10.cloned.1.call-start = ((), (), s32[]{:S(2)}) async-start(), calls=%async_computation.4 | async-start | bytes 2621440 | tf_op jit(solution)/shard_map/all_gather | solution.py:72
  136.5 5.5 %slice-start = ((f32[4096,258]{0,1:T(8,128)}), f32[4096,2]{0,1:T(2,128)S(1)}, s32[]{:S(2)}) async-start(f32[4096,258]{0,1:T(8,128)} %all-gather.6.cloned.1.call-done), calls=%async_computation.8 | async-start | bytes 65536 | tf_op jit(solution)/shard_map/split | solution.py:9
  205.3 13.2 %copy-start.1 = (f32[2048]{0:T(1024)S(1)}, f32[2048]{0:T(1024)}, u32[]{:S(2)}) copy-start(f32[2048]{0:T(1024)} %param.17) | copy-start | bytes 24580
  219.5 146.8 %all-gather.12.cloned.1.call-start = ((), (), s32[]{:S(2)}) async-start(), calls=%async_computation.5 | async-start | bytes 9437184 | tf_op jit(solution)/shard_map/all_gather | solution.py:75
  220.0 271.3 %all-gather.14.cloned.1.call-start = ((), (), s32[]{:S(2)}) async-start(), calls=%async_computation.6 | async-start | bytes 9437184 | tf_op jit(solution)/shard_map/all_gather | solution.py:79
  220.6 316.7 %reduce-scatter.2.cloned.1.call-start = ((), (), s32[]{:S(2)}) async-start(), calls=%async_computation.7 | async-start | bytes 2621440 | tf_op jit(solution)/shard_map/reduce_scatter | solution.py:81
Sparse Core Ops, SparseCore 0:
  9.5 51.7 all-gather.7
  63.5 72.9 all-gather.5
  219.6 20.1 all-gather.9
  241.8 124.4 all-gather.11
  368.2 123.1 all-gather.13
  508.0 29.3 reduce-scatter.1
